TPU v7x, 32 devices: a whole 2x2x4 slice. The times are simulated.
32 devices in a mesh: kv: 8 (over z, x), tp: 4 (over y, core).
Axes of the slice: x: 2, y: 2, z: 4, core: 2. Of those that a mesh axis runs over, the one named last changes fastest.
Arguments:
- tokens: bfloat16 [384, 2048], P(None, 'kv'), may hold values from -40 to 40
- norm_gain: float32 [2048], P('kv'), may hold values from 0.1 to 1.9
- w_query: bfloat16 [2048, 1024], P('kv', 'tp'), may hold values from -0.088388348 to 0.088388348
- w_key: bfloat16 [2048, 1024], P('kv', 'tp'), may hold values from -0.125 to 0.125
- w_value: bfloat16 [2048, 1024], P('kv', 'tp'), may hold values from -0.125 to 0.125
- w_gate: bfloat16 [2048, 16], replicated, may hold values from -0.125 to 0.125
- gate_bias: float32 [16], replicated, may hold values from -1 to 3
- w_out: bfloat16 [1024, 2048], P('tp', 'kv'), may hold values from -0.1875 to 0.1875
- keys_cache: bfloat16 [24, 4096, 1024], P(None, 'kv', 'tp'), may hold values from -512 to 512
- values_cache: bfloat16 [24, 4096, 1024], P(None, 'kv', 'tp'), may hold values from -6 to 6
- cum_gates: float32 [24, 16, 4096], P(None, 'tp', 'kv'), may hold values from -4496 to 0, as said below
- prior_len: int32 [24], replicated, may hold values from 2048 to 4074, as said below
- accepted: int32 [24], replicated, may hold values from 0 to 6
- parents: int32 [24, 16], replicated, may hold values from -1 to 14, as said below
Outputs:
- mixed_rows: bfloat16 [384, 2048], P('tp', 'kv')
- keys_out: bfloat16 [24, 4096, 1024], P(None, 'kv', 'tp')
- values_out: bfloat16 [24, 4096, 1024], P(None, 'kv', 'tp')
Inputs may be any that keep to these rules, and one draw needn't show every extreme that they name: parents[b, 0] = -1 and 0 <= parents[b, j] < j for later j. prior_len is at least half of 4096, and prior_len + accepted + 16 <= 4096. `cum_gates`: non-increasing along positions.
All inputs are finite; a program needn't handle non-finite values.
Results may differ from a plain program's by a relative error of at most 0.04.
Values may be sent and summed in bfloat16 or wider, within the bound.
A program may use at most 64 MiB of HBM per device.

v0:
```python
import jax
import jax.numpy as jnp
from jax import lax
from jax.sharding import PartitionSpec as P

D = 2048
HEAD = 64
PROPS = 16


masked_score = -1e30
norm_eps = 1e-06


def ancestry(parents):
    columns = jnp.arange(PROPS, dtype=jnp.int32)
    parent_link = (parents[:, :, None] == columns[None, None, :]).astype(jnp.float32)
    reached = jnp.eye(PROPS, dtype=jnp.float32)[None] + parent_link
    for squaring in range(PROPS.bit_length()):
        reached = jnp.minimum(
            jnp.einsum("bij,bjk->bik", reached, reached, precision=lax.Precision.HIGHEST), 1.0
        )
    return reached


def shards(
    tokens,
    norm_gain,
    w_query,
    w_key,
    w_value,
    w_gate,
    gate_bias,
    w_out,
    keys_cache,
    values_cache,
    cum_gates,
    prior_len,
    accepted,
    parents,
):
    row_count = tokens.shape[0]
    column_count = tokens.shape[1]
    seq_count = keys_cache.shape[0]
    length = keys_cache.shape[1]
    head_width = w_query.shape[1]
    head_count = head_width // HEAD
    kv_index = lax.axis_index("kv")
    tp_index = lax.axis_index("tp")
    floats = tokens.astype(jnp.float32)
    square_part = jnp.sum(floats * floats, axis=1)
    scaled = (floats * norm_gain).astype(jnp.bfloat16)
    gate_rows = lax.dynamic_slice_in_dim(w_gate, kv_index * column_count, column_count, 0)
    gate_cols = lax.dynamic_slice_in_dim(gate_rows, tp_index * head_count, head_count, 1)
    gate_part = jnp.dot(scaled, gate_cols, preferred_element_type=jnp.float32)
    bias_local = lax.dynamic_slice_in_dim(gate_bias, tp_index * head_count, head_count, 0)
    query_sum, key_sum, value_sum, gate_sum, square_sum = (
        lax.psum(
            jnp.dot(scaled, w_query, preferred_element_type=jnp.float32).astype(jnp.bfloat16), "kv"
        ).astype(jnp.float32),
        lax.psum(
            jnp.dot(scaled, w_key, preferred_element_type=jnp.float32).astype(jnp.bfloat16), "kv"
        ).astype(jnp.float32),
        lax.psum(
            jnp.dot(scaled, w_value, preferred_element_type=jnp.float32).astype(jnp.bfloat16), "kv"
        ).astype(jnp.float32),
        lax.psum(gate_part.astype(jnp.bfloat16), "kv").astype(jnp.float32),
        lax.psum(square_part.astype(jnp.bfloat16), "kv").astype(jnp.float32),
    )
    inv_rms = lax.rsqrt(square_sum / D + norm_eps)
    queries = (inv_rms[:, None] * query_sum).astype(jnp.bfloat16)
    new_keys = (inv_rms[:, None] * key_sum).astype(jnp.bfloat16)
    new_values = (inv_rms[:, None] * value_sum).astype(jnp.bfloat16)
    log_gates = jax.nn.log_sigmoid(inv_rms[:, None] * gate_sum + bias_local).reshape(
        seq_count, PROPS, head_count
    )
    reached = ancestry(parents)
    tree_gates = jnp.einsum("bij,bjh->bih", reached, log_gates, precision=lax.Precision.HIGHEST)
    filled = prior_len + accepted
    offset = kv_index * length
    local_last = filled - 1 - offset
    owner_mask = (local_last >= 0) & (local_last < length)
    index_last = jnp.broadcast_to(
        jnp.clip(local_last, 0, length - 1)[:, None, None], (seq_count, head_count, 1)
    )
    last_gate = jnp.take_along_axis(cum_gates, index_last, axis=2)[:, :, 0]
    prop_cum = last_gate[:, None, :] + tree_gates
    scale = HEAD ** (-0.5)
    query_four = queries.reshape(seq_count, PROPS, head_count, HEAD)
    keys_four = keys_cache.reshape(seq_count, length, head_count, HEAD)
    values_four = values_cache.reshape(seq_count, length, head_count, HEAD)
    newk_four = new_keys.reshape(seq_count, PROPS, head_count, HEAD)
    newv_four = new_values.reshape(seq_count, PROPS, head_count, HEAD)
    positions = offset + jnp.arange(length, dtype=jnp.int32)
    valid_keys = positions[None, :] < filled[:, None]
    scores = (
        jnp.einsum("bihd,bphd->bhip", query_four, keys_four, preferred_element_type=jnp.float32)
        * scale
    )
    scores = jnp.where(
        valid_keys[:, None, None, :], scores - cum_gates[:, :, None, :], masked_score
    )
    tree_scores = (
        jnp.einsum("bihd,bjhd->bhij", query_four, newk_four, preferred_element_type=jnp.float32)
        * scale
    )
    tree_scores = tree_scores - jnp.transpose(prop_cum, (0, 2, 1))[:, :, None, :]
    tree_live = (reached > 0.5)[:, None, :, :] & owner_mask[:, None, None, None]
    tree_scores = jnp.where(tree_live, tree_scores, masked_score)
    local_max = jnp.maximum(jnp.max(scores, axis=3), jnp.max(tree_scores, axis=3))
    weights = jnp.where(valid_keys[:, None, None, :], jnp.exp(scores - local_max[..., None]), 0.0)
    tree_weights = jnp.where(tree_live, jnp.exp(tree_scores - local_max[..., None]), 0.0)
    local_sum = jnp.sum(weights, axis=3) + jnp.sum(tree_weights, axis=3)
    local_values = jnp.einsum(
        "bhip,bphd->bhid",
        weights.astype(jnp.bfloat16),
        values_four,
        preferred_element_type=jnp.float32,
    )
    local_values = local_values + jnp.einsum(
        "bhij,bjhd->bhid",
        tree_weights.astype(jnp.bfloat16),
        newv_four,
        preferred_element_type=jnp.float32,
    )
    local_values = lax.optimization_barrier(local_values.astype(jnp.bfloat16)).astype(jnp.float32)
    top_score = lax.pmax(local_max, "kv")
    rescale = jnp.exp(local_max - top_score)
    grand_total, weighted = (
        lax.psum((rescale * local_sum).astype(jnp.bfloat16), "kv").astype(jnp.float32),
        lax.psum((rescale[..., None] * local_values).astype(jnp.bfloat16), "kv").astype(
            jnp.float32
        ),
    )
    result = weighted / grand_total[..., None]
    attended = (
        jnp.transpose(result, (0, 2, 1, 3)).reshape(row_count, head_width).astype(jnp.bfloat16)
    )
    partial_value = jnp.dot(attended, w_out, preferred_element_type=jnp.float32)
    mixed_rows = lax.psum_scatter(
        partial_value.astype(jnp.bfloat16), "tp", scatter_dimension=0, tiled=True
    )
    slot_index = positions[None, :] - filled[:, None]
    inside = (slot_index >= 0) & (slot_index < PROPS)
    selector = (slot_index[:, :, None] == jnp.arange(PROPS, dtype=jnp.int32)[None, None, :]).astype(
        jnp.bfloat16
    )
    placed_keys = jnp.einsum(
        "bpj,bjc->bpc",
        selector,
        new_keys.reshape(seq_count, PROPS, head_width),
        preferred_element_type=jnp.float32,
    ).astype(jnp.bfloat16)
    placed_values = jnp.einsum(
        "bpj,bjc->bpc",
        selector,
        new_values.reshape(seq_count, PROPS, head_width),
        preferred_element_type=jnp.float32,
    ).astype(jnp.bfloat16)
    keys_out = jnp.where(inside[:, :, None], placed_keys, keys_cache)
    values_out = jnp.where(inside[:, :, None], placed_values, values_cache)
    return (mixed_rows, keys_out, values_out)


def solution(mesh):
    placed = (
        P(None, "kv"),
        P("kv"),
        P("kv", "tp"),
        P("kv", "tp"),
        P("kv", "tp"),
        P(),
        P(),
        P("tp", "kv"),
        P(None, "kv", "tp"),
        P(None, "kv", "tp"),
        P(None, "tp", "kv"),
        P(),
        P(),
        P(),
    )
    return jax.shard_map(
        shards,
        mesh=mesh,
        in_specs=placed,
        out_specs=(P("tp", "kv"), P(None, "kv", "tp"), P(None, "kv", "tp")),
        check_vma=False,
    )
```

profile of v0, /device:TPU:0, one launch (start us, length us, event | category | flops | bytes accessed | tf_op | source)
XLA Modules:
  0.0 252.3 jit_solution(12036596136447176376)
XLA Ops:
  7.2 0.8 copy-done
  8.1 1.8 convolution_convert_fusion.1
  9.9 1.9 convolution_convert_fusion.2
  11.8 1.9 convolution_convert_fusion.3
  13.8 1.1 fusion.13
  14.9 0.7 compare_and_fusion.2
  15.9 2.4 gather_fusion
  18.5 0.9 convolution_convert_fusion.4
  19.3 23.2 %all-reduce = (bf16[384]{0:T(512)(128)(2,1)S(1)}, bf16[384,4]{0,1:T(4,128)(2,1)S(1)}) all-reduce(bf16[384]{0:T(512)(128)(2,1)S(1)} %fusion.13, bf16[384,4]{0,1:T(4,128)(2,1)S(1)} %convolution_convert_fusion.4), channel_id=1, replica_groups=mesh['kv'=8,'tp'=4] {'kv'}, use_global_device_ids=true, to_apply=%region_1.0 | all-reduce | flops 1920 | bytes 7680 | tf_op jit(solution)/shard_map/psum | solution.py:68
  43.0 0.4 convolution_minimum_fusion.4
  43.4 0.3 convolution_minimum_fusion.3
  43.7 0.3 convolution_minimum_fusion.2
  44.0 0.3 convolution_minimum_fusion.1
  44.3 0.3 compare_and_fusion
  44.7 0.4 convolution_add_fusion.1
  45.4 8.7 %copy.82 = bf16[24,512,256]{1,2,0:T(8,128)(2,1)} copy(bf16[24,512,256]{2,1,0:T(8,128)(2,1)} %param.22) | data formatting | bytes 12582912 | tf_op args[8]
  54.0 8.6 %copy.93 = bf16[24,512,256]{1,2,0:T(8,128)(2,1)} copy(bf16[24,512,256]{2,1,0:T(8,128)(2,1)} %param.23) | data formatting | bytes 12582912 | tf_op args[9]
  62.7 0.7 compare_and_fusion.1
  63.4 0.7 broadcast_subtract_fusion
  64.1 26.3 %all-reduce.7.cloned.1.call-done = (bf16[384,256]{1,0:T(8,128)(2,1)}, bf16[384,256]{1,0:T(8,128)(2,1)}, bf16[384,256]{1,0:T(8,128)(2,1)}) async-done(((bf16[384,256]{1,0:T(8,128)(2,1)}, bf16[384,256]{1,0:T(8,128)(2,1)}, bf16[384,256]{1,0:T(8,128)(2,1)}), (bf16[384,256]{1,0:T(8,128)(2,1)}, bf16[384,256]{1,0:T(8,128)(2,1)}, bf16[384,256]{1,0:T(8,128)(2,1)})) %all-reduce.7.cloned.1.call-update) | async-done | bytes 589840 | tf_op jit(solution)/shard_map/psum | solution.py:58
  90.4 1.9 multiply_convert_fusion.1
  92.3 0.2 reshape.281
  92.6 0.5 copy-done.6
  93.0 0.2 reshape.283
  93.3 0.3 fusion.17
  93.7 0.6 copy.88
  94.4 0.7 copy.92
  95.1 4.1 %fusion = (f32[24,4,16]{2,1,0:T(4,128)S(1)}, f32[24,4,16,512]{3,2,1,0:T(8,128)S(1)}) fusion(f32[24,4,512]{2,1,0:T(4,128)S(1)} %copy-done.1, pred[24,512]{1,0:T(8,128)(4,1)S(1)} %get-tuple-element.17, bf16[24,512,4,64]{1,3,2,0:T(8,128)(2,1)} %bitcast.31, bf16[24,16,4,64]{3,2,1,0:T(4,128)(2,1)} %copy-done.4), kind=kOutput, calls=%fused_computation.5 | convolution fusion | flops 103807488 | bytes 9848832 | tf_op jit(solution)/shard_map/bihd,bphd->bhip/dot_general | solution.py:97
  99.3 0.7 copy.94
  100.0 36.4 %pmax.7 = f32[24,4,16]{2,1,0:T(4,128)} all-reduce(f32[24,4,16]{2,1,0:T(4,128)S(1)} %max.25), channel_id=1, replica_groups=mesh['kv'=8,'tp'=4] {'kv'}, use_global_device_ids=true, to_apply=%region_7.8 | all-reduce | flops 1536 | bytes 12288 | tf_op jit(solution)/shard_map/pmax | solution.py:127
  136.4 2.6 %fusion.1 = f32[24,4,16]{2,1,0:T(4,128)} fusion(f32[24,4,16,512]{3,2,1,0:T(8,128)S(1)} %get-tuple-element.22, f32[24,4,16]{2,1,0:T(4,128)S(1)} %max.25, f32[24,4,512]{2,1,0:T(4,128)S(1)} %copy-done.1, pred[24,512]{1,0:T(8,128)(4,1)} %copy-done.16), kind=kLoop, calls=%fused_computation.6 | loop fusion | flops 4717056 | bytes 3366912 | tf_op jit(solution)/shard_map/reduce_sum | solution.py:113
  139.0 1.5 fusion.24
  140.5 1.5 copy.97
  142.0 2.4 copy.95
  144.3 5.5 %fusion.3 = f32[24,4,16,64]{3,2,1,0:T(8,128)} fusion(bf16[24,512,4,64]{1,3,2,0:T(8,128)(2,1)} %bitcast.32, f32[24,4,16,512]{3,2,1,0:T(8,128)S(1)} %get-tuple-element.22, f32[24,4,16]{2,1,0:T(4,128)S(1)} %max.25, f32[24,4,512]{2,1,0:T(4,128)S(1)} %copy-done.1, pred[24,512]{1,0:T(8,128)(4,1)} %copy-done.16), kind=kOutput, calls=%fused_computation.8 | convolution fusion | flops 105381888 | bytes 10045440 | tf_op jit(solution)/shard_map/bhip,bphd->bhid/dot_general | solution.py:114
  149.8 1.2 reshape.286
  151.0 1.6 fusion.11
  152.6 0.9 multiply_convert_fusion.4
  153.5 1.0 multiply_convert_fusion
  154.7 8.3 %convert_select_fusion = bf16[24,512,256]{2,1,0:T(8,128)(2,1)} fusion(bf16[24,512,256]{2,1,0:T(8,128)(2,1)} %param.23, pred[24,512]{1,0:T(8,128)(4,1)S(1)} %copy-done.15, bf16[24,16,256]{2,1,0:T(8,128)(2,1)S(1)} %bitcast.34, s32[24,512]{1,0:T(8,128)S(1)} %copy-done.9), kind=kOutput, calls=%fused_computation.1 | convolution fusion | flops 107151360 | bytes 12840960 | tf_op jit(solution)/shard_map/bpj,bjc->bpc/dot_general | solution.py:154
  162.9 33.2 %psum.55 = bf16[24,4,16]{2,1,0:T(4,128)(2,1)S(1)} all-reduce(bf16[24,4,16]{2,1,0:T(4,128)(2,1)S(1)} %get-tuple-element.8), channel_id=1, replica_groups=mesh['kv'=8,'tp'=4] {'kv'}, use_global_device_ids=true, to_apply=%region_12.13 | all-reduce | flops 1536 | bytes 6144 | tf_op jit(solution)/shard_map/psum | solution.py:130
  196.1 27.8 %all-reduce.5.cloned.1.call-done = bf16[24,4,16,64]{3,2,1,0:T(8,128)(2,1)} async-done(((bf16[24,4,16,64]{3,2,1,0:T(8,128)(2,1)}), bf16[24,4,16,64]{3,2,1,0:T(8,128)(2,1)}) %all-reduce.5.cloned.1.call-update) | async-done | bytes 196624 | tf_op jit(solution)/shard_map/psum | solution.py:131
  223.9 1.3 fusion.15
  225.2 0.2 copy.98
  225.4 0.3 convert_element_type.125
  225.7 0.9 convolution_convert_fusion
  226.6 8.2 %convert_select_fusion.1 = bf16[24,512,256]{2,1,0:T(8,128)(2,1)} fusion(bf16[24,512,256]{2,1,0:T(8,128)(2,1)} %param.22, pred[24,512]{1,0:T(8,128)(4,1)S(1)} %copy-done.15, bf16[24,16,256]{2,1,0:T(8,128)(2,1)S(1)} %bitcast.33, s32[24,512]{1,0:T(8,128)S(1)} %copy-done.9), kind=kOutput, calls=%fused_computation.2 | convolution fusion | flops 107151360 | bytes 12840960 | tf_op jit(solution)/shard_map/bpj,bjc->bpc/dot_general | solution.py:148
  234.8 11.0 %reduce-scatter.2.cloned.1.call-done = bf16[96,256]{1,0:T(8,128)(2,1)} async-done(((bf16[384,256]{1,0:T(8,128)(2,1)}), bf16[96,256]{1,0:T(8,128)(2,1)}) %reduce-scatter.2.cloned.1.call-update) | async-done | bytes 49168 | tf_op jit(solution)/shard_map/reduce_scatter | solution.py:140
  (67 shorter events, 1.5 us)
Async XLA Ops:
  7.2 0.9 copy-start
  7.2 8.6 %copy-start.1 = (f32[24,4,512]{2,1,0:T(4,128)S(1)}, f32[24,4,512]{2,1,0:T(4,128)}, u32[]{:S(2)}) copy-start(f32[24,4,512]{2,1,0:T(4,128)} %param.24) | copy-start | bytes 589828
  7.2 83.2 %all-reduce.7.cloned.1.call-start = ((), (), s32[]{:S(2)}) async-start(), calls=%async_computation.3 | async-start | bytes 1179648 | tf_op jit(solution)/shard_map/psum | solution.py:58
  13.7 210.2 %all-reduce.5.cloned.1.call-start = ((), (), s32[]{:S(2)}) async-start(), calls=%async_computation.1 | async-start | bytes 786432 | tf_op jit(solution)/shard_map/psum | solution.py:131
  15.8 2.6 %copy-start.5 = (bf16[384,256]{1,0:T(8,128)(2,1)S(1)}, bf16[384,256]{1,0:T(8,128)(2,1)}, u32[]{:S(2)}) copy-start(bf16[384,256]{1,0:T(8,128)(2,1)} %param.14) | copy-start | bytes 589828
  15.8 2.6 %copy-start.17 = (f32[256]{0:T(256)S(1)}, f32[256]{0:T(256)}, u32[]{:S(2)}) copy-start(f32[256]{0:T(256)} %param.15) | copy-start | bytes 3076
  15.9 26.7 %copy-start.19 = (f32[16]{0:T(128)S(1)}, f32[16]{0:T(128)}, u32[]{:S(2)}) copy-start(f32[16]{0:T(128)} %param.20) | copy-start | bytes 196
  15.9 27.0 %copy-start.18 = (s32[24,16]{0,1:T(8,128)S(1)}, s32[24,16]{0,1:T(8,128)}, u32[]{:S(2)}) copy-start(s32[24,16]{0,1:T(8,128)} %param.27) | copy-start | bytes 4612
  45.4 48.8 %copy-start.10 = (pred[24,16,16]{0,2,1:T(8,128)(4,1)}, pred[24,16,16]{0,2,1:T(8,128)(4,1)S(1)}, u32[]{:S(2)}) copy-start(pred[24,16,16]{0,2,1:T(8,128)(4,1)S(1)} %copy.85) | copy-start | bytes 18436
  63.4 35.8 %copy-start.16 = (pred[24,512]{1,0:T(8,128)(4,1)}, pred[24,512]{1,0:T(8,128)(4,1)S(1)}, u32[]{:S(2)}) copy-start(pred[24,512]{1,0:T(8,128)(4,1)S(1)} %get-tuple-element.17) | copy-start | bytes 36868
  92.3 0.7 copy-start.6
  92.6 0.8 copy-start.4
  94.2 0.9 copy-start.2
  95.1 4.1 %copy-start.12 = (f32[24,4,16]{2,1,0:T(4,128)S(1)}, f32[24,4,16]{2,1,0:T(4,128)}, u32[]{:S(2)}) copy-start(f32[24,4,16]{2,1,0:T(4,128)} %copy.92) | copy-start | bytes 18436
  136.4 2.6 %copy-start.3 = (f32[24,4,16,16]{0,3,2,1:T(8,128)S(1)}, f32[24,4,16,16]{0,3,2,1:T(8,128)}, u32[]{:S(2)}) copy-start(f32[24,4,16,16]{0,3,2,1:T(8,128)} %copy-done.2) | copy-start | bytes 294916
  136.4 2.6 %copy-start.11 = (pred[24,16,16]{0,2,1:T(8,128)(4,1)S(1)}, pred[24,16,16]{0,2,1:T(8,128)(4,1)}, u32[]{:S(2)}) copy-start(pred[24,16,16]{0,2,1:T(8,128)(4,1)} %copy-done.10) | copy-start | bytes 18436
  136.4 2.6 %copy-start.13 = (f32[24,4,16]{0,2,1:T(8,128)S(1)}, f32[24,4,16]{0,2,1:T(8,128)}, u32[]{:S(2)}) copy-start(f32[24,4,16]{0,2,1:T(8,128)} %copy.94) | copy-start | bytes 18436
  149.8 4.8 %copy-start.8 = (bf16[384,256]{1,0:T(8,128)(2,1)S(1)}, bf16[384,256]{1,0:T(8,128)(2,1)}, u32[]{:S(2)}) copy-start(bf16[384,256]{1,0:T(8,128)(2,1)} %get-tuple-element.18) | copy-start | bytes 589828
  149.8 4.8 %copy-start.9 = (s32[24,512]{1,0:T(8,128)S(1)}, s32[24,512]{1,0:T(8,128)}, u32[]{:S(2)}) copy-start(s32[24,512]{1,0:T(8,128)} %broadcast_subtract_fusion) | copy-start | bytes 147460
  149.8 4.8 %copy-start.15 = (pred[24,512]{1,0:T(8,128)(4,1)S(1)}, pred[24,512]{1,0:T(8,128)(4,1)}, u32[]{:S(2)}) copy-start(pred[24,512]{1,0:T(8,128)(4,1)} %get-tuple-element.16) | copy-start | bytes 36868
  154.6 91.2 %reduce-scatter.2.cloned.1.call-start = ((), (), s32[]{:S(2)}) async-start(), calls=%async_computation.2 | async-start | bytes 245760 | tf_op jit(solution)/shard_map/reduce_scatter | solution.py:140
  154.7 71.0 %copy-start.14 = (bf16[256,256]{1,0:T(8,128)(2,1)S(1)}, bf16[256,256]{1,0:T(8,128)(2,1)}, u32[]{:S(2)}) copy-start(bf16[256,256]{1,0:T(8,128)(2,1)} %param.21) | copy-start | bytes 393220
  162.9 63.6 %copy-start.7 = (bf16[384,256]{1,0:T(8,128)(2,1)S(1)}, bf16[384,256]{1,0:T(8,128)(2,1)}, u32[]{:S(2)}) copy-start(bf16[384,256]{1,0:T(8,128)(2,1)} %copy-done.6) | copy-start | bytes 589828
Sparse Core Ops, SparseCore 0:
  13.8 76.5 all-reduce.6
  154.7 69.1 all-reduce.4
  226.9 18.7 reduce-scatter.1
where the time goes:
time: 254 us; the launch traced here: 252 us
  blocking collectives  92.9 us (37%)
  waiting for transfers between devices  65.1 us (26%)
  matrix products  37.5 us (15%)
  local copies, waits for them, and re-layouts  29.7 us (12%)
  between operations  14.2 us (6%)
  other arithmetic  12.7 us (5%)
    pmax x1, blocking collectives, shards(): top_score = lax.pmax(local_max, 'kv')  36.4 us
    psum x1, blocking collectives, shards(): lax.psum((rescale * local_sum).astype(jnp.bfloat16), 'kv')  33.2 us
    psum x1, waiting for transfers between devices, shards(): lax.psum((rescale[..., None] * local_values).astype(jnp.bfloat16), 'kv')  27.8 us
    psum x1, waiting for transfers between devices, shards(): lax.psum(jnp.dot(scaled, w_query, preferred_element_type=jnp.float32).ast...  26.3 us
    psum x1, blocking collectives, shards(): lax.psum(square_part.astype(jnp.bfloat16), 'kv').astype(jnp.float32)  23.2 us
    unnamed x45, local copies, waits for them, and re-layouts  18.8 us
    reduce_scatter x1, waiting for transfers between devices, shards(): lax.psum_scatter(partial_value.astype(jnp.bfloat16), 'tp', scatter_dimens...  11 us
    dot_general x1, matrix products, shards(): jnp.einsum('bpj,bjc->bpc', selector, new_values.reshape(seq_count, PROPS,...  8.26 us
  transfers between devices with their start and end apart: 3, of which 3 were waited for; matrix products, arithmetic and copies ran while one was open for 17% of the time, Pallas kernels for 0%

commit v1 on v0

v1 whole, which is shorter than its diff:
```python
import functools

import jax
import jax.numpy as jnp
from jax import lax
from jax.experimental import pallas as pl
from jax.experimental.pallas import tpu as pltpu
from jax.sharding import PartitionSpec as P

HEAD = 64
PROPS = 16
LANES = 128
SQUARE_LANE = 96
masked_score = -1e30
norm_eps = 1e-06
MESH = pl.DeviceIdType.MESH
HIGHEST = lax.Precision.HIGHEST
f32, bf16, i32 = jnp.float32, jnp.bfloat16, jnp.int32


def iota(shape, axis):
    return lax.broadcasted_iota(i32, shape, axis)


def split3(x):
    hi = x.astype(bf16).astype(f32)
    mid = (x - hi).astype(bf16).astype(f32)
    return hi, mid, x - hi - mid


def contract_last(a, b, precision=None):
    return lax.dot_general(
        a, b, (((1,), (1,)), ((), ())), preferred_element_type=f32, precision=precision
    )


def project_kernel(
    n_kv,
    heads,
    tokens_ref,
    gain_ref,
    wq_ref,
    wk_ref,
    wv_ref,
    wg_ref,
    bias_ref,
    out_ref,
    part,
    arrived,
    gathered,
    mine,
    send_a,
    recv_a,
    send_b,
    recv_b,
):
    me = lax.axis_index("kv")
    tp = lax.axis_index("tp")
    chunk_rows, depth = tokens_ref.shape[1:]
    width = heads * HEAD
    barrier = pltpu.get_barrier_semaphore()
    for d in range(1, n_kv):
        pl.semaphore_signal(
            barrier, inc=1, device_id={"kv": lax.rem(me + d, n_kv)}, device_id_type=MESH
        )

    total_heads = wg_ref.shape[1]
    lane = iota((total_heads, LANES), 1)
    pick = (iota((total_heads, LANES), 0) == tp * heads + lane % 32) & (lane % 32 < heads) & (lane < 96)
    pick = jnp.where(pick, 1.0, 0.0)
    gate_w = wg_ref[pl.ds(pl.multiple_of(me * depth, depth), depth), :]
    gate_w = jnp.dot(gate_w, pick.astype(bf16), preferred_element_type=f32).astype(bf16)

    def partial_sums(floats):
        scaled = (floats * gain_ref[...]).astype(bf16)
        square = jnp.sum(floats * floats, axis=1, keepdims=True)
        gates = jnp.dot(scaled, gate_w, preferred_element_type=f32)
        gates = jnp.where(iota(gates.shape, 1) == SQUARE_LANE, square, gates)
        products = [
            jnp.dot(scaled, w[...], preferred_element_type=f32).astype(bf16)
            for w in (wq_ref, wk_ref, wv_ref)
        ]
        return products + [gates.astype(bf16)]

    edges = [0, width, 2 * width, 3 * width, 3 * width + LANES]
    if chunk_rows % 16 == 0:
        floats = tokens_ref[...].reshape(n_kv * chunk_rows, depth).astype(f32)
        for piece, low, high in zip(partial_sums(floats), edges[:-1], edges[1:]):
            part[:, :, low:high] = piece.reshape(n_kv, chunk_rows, high - low)
    else:

        def one(c, carry):
            for piece, low, high in zip(
                partial_sums(tokens_ref[c].astype(f32)), edges[:-1], edges[1:]
            ):
                part[c, :, low:high] = piece
            return carry

        lax.fori_loop(0, n_kv, one, 0)

    pl.semaphore_wait(barrier, n_kv - 1)
    copies = []
    for d in range(1, n_kv):
        peer = lax.rem(me + d, n_kv)
        copy = pltpu.make_async_remote_copy(
            src_ref=part.at[peer],
            dst_ref=arrived.at[d - 1],
            send_sem=send_a.at[d - 1],
            recv_sem=recv_a.at[d - 1],
            device_id={"kv": peer},
            device_id_type=MESH,
        )
        copy.start()
        copies.append(copy)
    total = part[me].astype(f32)
    for d in range(1, n_kv):
        copies[d - 1].wait_recv()
        total = total + arrived[d - 1].astype(f32)
    tail = total[:, 3 * width :]
    tail_lane = iota(tail.shape, 1)
    square = jnp.sum(jnp.where(tail_lane == SQUARE_LANE, tail, 0.0), axis=1, keepdims=True)
    inv_rms = lax.rsqrt(square / (n_kv * depth) + norm_eps)
    bias = jnp.dot(
        jnp.broadcast_to(bias_ref[...], (8, total_heads)),
        pick,
        preferred_element_type=f32,
        precision=HIGHEST,
    )[0:1]
    pre = inv_rms * tail + bias
    log_gates = jnp.minimum(pre, 0.0) - jnp.log1p(jnp.exp(-jnp.abs(pre)))
    hi, mid, low = split3(log_gates)
    packed = jnp.where(tail_lane < 32, hi, jnp.where(tail_lane < 64, mid, low))
    packed = jnp.where((tail_lane % 32 < heads) & (tail_lane < 96), packed, 0.0)
    mine[:, : 3 * width] = (inv_rms * total[:, : 3 * width]).astype(bf16)
    mine[:, 3 * width :] = packed.astype(bf16)
    back = []
    for d in range(1, n_kv):
        copy = pltpu.make_async_remote_copy(
            src_ref=mine,
            dst_ref=gathered.at[me],
            send_sem=send_b.at[d - 1],
            recv_sem=recv_b.at[d - 1],
            device_id={"kv": lax.rem(me + d, n_kv)},
            device_id_type=MESH,
        )
        copy.start()
        back.append(copy)
    out_ref[me] = mine[...]
    for d in range(1, n_kv):
        source = lax.rem(me + n_kv - d, n_kv)
        back[d - 1].wait_recv()
        out_ref[source] = gathered[source]
    for copy in copies + back:
        copy.wait_send()


def attend_kernel(
    heads, prior_s, accepted_s, proj_ref, parents_ref, k_ref, v_ref, cum_ref, ko_ref, vo_ref, out_ref
):
    group = k_ref.shape[0]
    length = k_ref.shape[1]
    width = heads * HEAD
    rows = group * PROPS
    score_rows = heads * PROPS
    offset = lax.axis_index("kv") * length
    step = pl.program_id(0)

    row = iota((rows, rows), 0)
    column = iota((rows, rows), 1)
    parent = parents_ref[...]
    link = (parent + (row // PROPS) * PROPS == column) & (parent >= 0)
    reached = jnp.where(link | (row == column), 1.0, 0.0)
    for squaring in range((PROPS - 1).bit_length()):
        reached = jnp.minimum(
            jnp.dot(reached.astype(bf16), reached.astype(bf16), preferred_element_type=f32), 1.0
        )
    tree_gates = jnp.dot(
        reached.astype(bf16), proj_ref[:, 3 * width :], preferred_element_type=f32
    )
    lane = iota((score_rows, LANES), 1)
    row_head = iota((score_rows, LANES), 0) // PROPS
    gate_pick = jnp.where((lane % 32 == row_head) & (lane < 96), 1.0, 0.0)
    same_head = iota((score_rows, width), 0) // PROPS == iota((score_rows, width), 1) // HEAD
    position = iota((score_rows, length), 1)
    window = 2 * PROPS
    for b in range(group):
        span = slice(b * PROPS, (b + 1) * PROPS)
        seq = step * group + b
        limit = prior_s[seq] + accepted_s[seq] - offset
        owner = jnp.where((limit >= 1) & (limit <= length), 1.0, 0.0)
        new_k = proj_ref[span, width : 2 * width]
        new_v = proj_ref[span, 2 * width : 3 * width]
        query = jnp.concatenate([proj_ref[span, :width]] * heads, axis=0).astype(f32)
        query = (jnp.where(same_head, query, 0.0) * HEAD ** (-0.5)).astype(bf16)
        cum = jnp.concatenate(
            [
                jnp.broadcast_to(cum_ref[b, h : h + 1, :], (PROPS, length))
                for h in range(heads)
            ],
            axis=0,
        )
        valid = position < limit
        scores = jnp.where(valid, contract_last(query, k_ref[b]) - cum, masked_score)
        last = jnp.sum(jnp.where(position == limit - 1, cum, 0.0), axis=1, keepdims=True)
        prop_cum = last + contract_last(gate_pick, tree_gates[span], HIGHEST)
        live = jnp.concatenate([reached[span, span]] * heads, axis=0) * owner > 0.5
        tree = jnp.where(live, contract_last(query, new_k) - prop_cum, masked_score)
        top = jnp.maximum(
            jnp.max(scores, axis=1, keepdims=True), jnp.max(tree, axis=1, keepdims=True)
        )
        weights = jnp.where(valid, jnp.exp(scores - top), 0.0)
        tree_weights = jnp.where(live, jnp.exp(tree - top), 0.0)
        total = jnp.sum(weights, axis=1, keepdims=True) + jnp.sum(
            tree_weights, axis=1, keepdims=True
        )
        values = jnp.dot(weights.astype(bf16), v_ref[b], preferred_element_type=f32)
        values = values + jnp.dot(tree_weights.astype(bf16), new_v, preferred_element_type=f32)
        values = jnp.where(same_head, values, 0.0)
        t_hi, t_mid, t_low = split3(top)
        s_hi, s_mid, s_low = split3(total)
        part = lane // 16
        packed = jnp.where(
            part == 0,
            t_hi,
            jnp.where(
                part == 1, t_mid, jnp.where(part == 2, t_low, jnp.where(part == 3, s_hi, s_mid))
            ),
        )
        packed = jnp.where((lane % 16 == row_head) & (part < 5), packed, 0.0)
        picked_values = values[:PROPS]
        picked_packed = packed[:PROPS]
        for h in range(1, heads):
            picked_values = picked_values + values[h * PROPS : (h + 1) * PROPS]
            picked_packed = picked_packed + packed[h * PROPS : (h + 1) * PROPS]
        out_ref[span, :width] = picked_values.astype(bf16)
        out_ref[span, width:] = picked_packed.astype(bf16)

        start = pl.multiple_of(jnp.clip(limit, 0, length - window) // PROPS * PROPS, PROPS)
        select = start + iota((window, PROPS), 0) - limit == iota((window, PROPS), 1)
        select = jnp.where(select, 1.0, 0.0).astype(bf16)
        slot = start + iota((window, width), 0) - limit
        inside = (slot >= 0) & (slot < PROPS)
        for source, target, fresh in ((k_ref, ko_ref, new_k), (v_ref, vo_ref, new_v)):
            target[b] = source[b]
            placed = jnp.dot(select, fresh, preferred_element_type=f32)
            old = source[b, pl.ds(start, window), :].astype(f32)
            target[b, pl.ds(start, window), :] = jnp.where(inside, placed, old).astype(bf16)


def combine_kernel(
    n_kv,
    n_tp,
    heads,
    parts_ref,
    w_ref,
    out_ref,
    arrived,
    mine,
    gathered,
    partial,
    landed,
    send_a,
    recv_a,
    send_b,
    recv_b,
    send_c,
    recv_c,
):
    me = lax.axis_index("kv")
    tp = lax.axis_index("tp")
    width = heads * HEAD
    chunk_rows = parts_ref.shape[1]
    share = n_kv // n_tp
    barrier = pltpu.get_barrier_semaphore()
    for d in range(1, n_kv):
        pl.semaphore_signal(
            barrier, inc=1, device_id={"kv": lax.rem(me + d, n_kv)}, device_id_type=MESH
        )
    for d in range(1, n_tp):
        pl.semaphore_signal(
            barrier, inc=1, device_id={"tp": lax.rem(tp + d, n_tp)}, device_id_type=MESH
        )
    pl.semaphore_wait(barrier, n_kv - 1 + n_tp - 1)
    first = []
    for d in range(1, n_kv):
        peer = lax.rem(me + d, n_kv)
        copy = pltpu.make_async_remote_copy(
            src_ref=parts_ref.at[peer],
            dst_ref=arrived.at[d - 1],
            send_sem=send_a.at[d - 1],
            recv_sem=recv_a.at[d - 1],
            device_id={"kv": peer},
            device_id_type=MESH,
        )
        copy.start()
        first.append(copy)
    lane = iota((LANES, width), 0)
    fits = lane % 16 == iota((LANES, width), 1) // HEAD
    spread_top = jnp.where(fits & (lane < 48), 1.0, 0.0).astype(bf16)
    spread_sum = jnp.where(fits & (lane >= 48) & (lane < 80), 1.0, 0.0).astype(bf16)

    def unpack(block):
        packed = block[:, width:]
        return (
            jnp.dot(packed, spread_top, preferred_element_type=f32),
            jnp.dot(packed, spread_sum, preferred_element_type=f32),
            block[:, :width].astype(f32),
        )

    top, sums, values = unpack(parts_ref[me])
    for d in range(1, n_kv):
        first[d - 1].wait_recv()
        other_top, other_sums, other_values = unpack(arrived[d - 1])
        new_top = jnp.maximum(top, other_top)
        here, there = jnp.exp(top - new_top), jnp.exp(other_top - new_top)
        sums = here * sums + there * other_sums
        values = here * values + there * other_values
        top = new_top
    mine[...] = (values / sums).astype(bf16)
    second = []
    for d in range(1, n_kv):
        copy = pltpu.make_async_remote_copy(
            src_ref=mine,
            dst_ref=gathered.at[me],
            send_sem=send_b.at[d - 1],
            recv_sem=recv_b.at[d - 1],
            device_id={"kv": lax.rem(me + d, n_kv)},
            device_id_type=MESH,
        )
        copy.start()
        second.append(copy)
    gathered[me] = mine[...]
    for copy in second:
        copy.wait_recv()
    if chunk_rows % 16 == 0:
        attended = gathered[...].reshape(n_kv * chunk_rows, width)
        product = jnp.dot(attended, w_ref[...], preferred_element_type=f32).astype(bf16)
        partial[...] = product.reshape(partial.shape)
    else:

        def one(c, carry):
            partial[c] = jnp.dot(gathered[c], w_ref[...], preferred_element_type=f32).astype(bf16)
            return carry

        lax.fori_loop(0, n_kv, one, 0)
    third = []
    for d in range(1, n_tp):
        peer = lax.rem(tp + d, n_tp)
        copy = pltpu.make_async_remote_copy(
            src_ref=partial.at[pl.ds(peer * share, share)],
            dst_ref=landed.at[d - 1],
            send_sem=send_c.at[d - 1],
            recv_sem=recv_c.at[d - 1],
            device_id={"tp": peer},
            device_id_type=MESH,
        )
        copy.start()
        third.append(copy)
    total = partial[pl.ds(tp * share, share)].astype(f32)
    for d in range(1, n_tp):
        third[d - 1].wait_recv()
        total = total + landed[d - 1].astype(f32)
    out_ref[...] = total.astype(bf16)
    for copy in first + second + third:
        copy.wait_send()


def shards(
    n_kv,
    n_tp,
    tokens,
    norm_gain,
    w_query,
    w_key,
    w_value,
    w_gate,
    gate_bias,
    w_out,
    keys_cache,
    values_cache,
    cum_gates,
    prior_len,
    accepted,
    parents,
):
    row_count, depth = tokens.shape
    seq_count, length, width = keys_cache.shape
    heads = width // HEAD
    chunk_rows = row_count // n_kv
    columns = w_out.shape[1]
    vmem = pl.BlockSpec(memory_space=pltpu.VMEM)
    dma = pltpu.SemaphoreType.DMA
    proj_width = 3 * width + LANES
    out_width = width + LANES

    projected = pl.pallas_call(
        functools.partial(project_kernel, n_kv, heads),
        out_shape=jax.ShapeDtypeStruct((n_kv, chunk_rows, proj_width), bf16),
        in_specs=[vmem] * 7,
        out_specs=vmem,
        scratch_shapes=[
            pltpu.VMEM((n_kv, chunk_rows, proj_width), bf16),
            pltpu.VMEM((n_kv - 1, chunk_rows, proj_width), bf16),
            pltpu.VMEM((n_kv, chunk_rows, proj_width), bf16),
            pltpu.VMEM((chunk_rows, proj_width), bf16),
        ]
        + [dma((n_kv - 1,))] * 4,
        compiler_params=pltpu.CompilerParams(collective_id=0, has_side_effects=True),
        name="project",
    )(
        tokens.reshape(n_kv, chunk_rows, depth),
        norm_gain.reshape(1, depth),
        w_query,
        w_key,
        w_value,
        w_gate,
        gate_bias.reshape(1, -1),
    )
    projected = projected.reshape(row_count, proj_width)

    group = next(g for g in (4, 3, 2, 1) if seq_count % g == 0)
    rows = group * PROPS
    cache_spec = pl.BlockSpec((group, length, width), lambda s, *_: (s, 0, 0))
    keys_out, values_out, parts = pl.pallas_call(
        functools.partial(attend_kernel, heads),
        out_shape=(
            jax.ShapeDtypeStruct(keys_cache.shape, bf16),
            jax.ShapeDtypeStruct(values_cache.shape, bf16),
            jax.ShapeDtypeStruct((row_count, out_width), bf16),
        ),
        grid_spec=pltpu.PrefetchScalarGridSpec(
            num_scalar_prefetch=2,
            grid=(seq_count // group,),
            in_specs=[
                pl.BlockSpec((rows, proj_width), lambda s, *_: (s, 0)),
                pl.BlockSpec((rows, 1), lambda s, *_: (s, 0)),
                cache_spec,
                cache_spec,
                pl.BlockSpec((group, heads, length), lambda s, *_: (s, 0, 0)),
            ],
            out_specs=[
                cache_spec,
                cache_spec,
                pl.BlockSpec((rows, out_width), lambda s, *_: (s, 0)),
            ],
        ),
        name="attend",
    )(
        prior_len,
        accepted,
        projected,
        parents.reshape(row_count, 1),
        keys_cache,
        values_cache,
        cum_gates,
    )

    mixed = pl.pallas_call(
        functools.partial(combine_kernel, n_kv, n_tp, heads),
        out_shape=jax.ShapeDtypeStruct((n_kv // n_tp, chunk_rows, columns), bf16),
        in_specs=[vmem] * 2,
        out_specs=vmem,
        scratch_shapes=[
            pltpu.VMEM((n_kv - 1, chunk_rows, out_width), bf16),
            pltpu.VMEM((chunk_rows, width), bf16),
            pltpu.VMEM((n_kv, chunk_rows, width), bf16),
            pltpu.VMEM((n_kv, chunk_rows, columns), bf16),
            pltpu.VMEM((n_tp - 1, n_kv // n_tp, chunk_rows, columns), bf16),
        ]
        + [dma((n_kv - 1,))] * 4
        + [dma((n_tp - 1,))] * 2,
        compiler_params=pltpu.CompilerParams(collective_id=1, has_side_effects=True),
        name="combine",
    )(parts.reshape(n_kv, chunk_rows, out_width), w_out)
    return (mixed.reshape(row_count // n_tp, columns), keys_out, values_out)


def solution(mesh):
    placed = (
        P(None, "kv"),
        P("kv"),
        P("kv", "tp"),
        P("kv", "tp"),
        P("kv", "tp"),
        P(),
        P(),
        P("tp", "kv"),
        P(None, "kv", "tp"),
        P(None, "kv", "tp"),
        P(None, "tp", "kv"),
        P(),
        P(),
        P(),
    )
    return jax.shard_map(
        functools.partial(shards, mesh.shape["kv"], mesh.shape["tp"]),
        mesh=mesh,
        in_specs=placed,
        out_specs=(P("tp", "kv"), P(None, "kv", "tp"), P(None, "kv", "tp")),
        check_vma=False,
    )
```

time: 254 us -> 89.6 us (0.35)
  blocking collectives: 92.9 us -> 0 us
  Pallas kernels: 0 us -> 83.8 us
  waiting for transfers between devices: 65.1 us -> 0 us
  matrix products: 37.5 us -> 0 us
  local copies, waits for them, and re-layouts: 29.7 us -> 4.85 us
  between operations: 14.2 us -> 0.65 us
  other arithmetic: 12.7 us -> 0 us
    pallas_call x0 -> x3, Pallas kernels: none -> 83.8 us  [the longest x1 37.2 us: shards(): pl.pallas_call(functools.partial(project_kernel, n_kv, heads), out_shape=...]
    psum x2 -> x0, blocking collectives: 56.4 us -> none  [the longest x1 33.2 us: shards(): lax.psum((rescale * local_sum).astype(jnp.bfloat16), 'kv')]
    psum x2 -> x0, waiting for transfers between devices: 54.1 us -> none  [the longest x1 27.8 us: shards(): lax.psum((rescale[..., None] * local_values).astype(jnp.bfloat16), 'kv')]
    dot_general x17 -> x0, matrix products: 37.5 us -> none  [the longest x1 8.26 us: shards(): jnp.einsum('bpj,bjc->bpc', selector, new_values.reshape(seq_count, PROPS,...]
    pmax x1 -> x0, blocking collectives: 36.4 us -> none  [shards(): top_score = lax.pmax(local_max, 'kv')]
    unnamed x45 -> x3, local copies, waits for them, and re-layouts: 18.8 us -> 4.03 us
    reduce_scatter x1 -> x0, waiting for transfers between devices: 11 us -> none  [shards(): lax.psum_scatter(partial_value.astype(jnp.bfloat16), 'tp', scatter_dimens...]
    reduce_sum x3 -> x0, other arithmetic: 5.16 us -> none  [the longest x2 4.09 us: shards(): local_sum = jnp.sum(weights, axis=3) + jnp.sum(tree_weights, axis=3)]
  transfers between devices with their start and end apart: 3 -> 0, of which waited for: 3 -> 0; matrix products, arithmetic and copies ran while one was open for 17% -> 0% of each run, Pallas kernels for 0% -> 0%
where the time goes in v1:
time: 89.6 us; the launch traced here: 89.3 us
  Pallas kernels  83.8 us (94%)
  local copies, waits for them, and re-layouts  4.85 us (5%)
    pallas_call x1, Pallas kernels, shards(): pl.pallas_call(functools.partial(project_kernel, n_kv, heads), out_shape=...  37.2 us
    pallas_call x1, Pallas kernels, shards(): pl.pallas_call(functools.partial(combine_kernel, n_kv, n_tp, heads), out_...  26.5 us
    pallas_call x1, Pallas kernels, shards(): pl.pallas_call(functools.partial(attend_kernel, heads), out_shape=(jax.Sh...  20.1 us
    unnamed x3, local copies, waits for them, and re-layouts  4.03 us

profile of v1, /device:TPU:0, one launch (start us, length us, event | category | flops | bytes accessed | tf_op | source)
XLA Modules:
  0.0 89.3 jit_solution(579256782004015603)
XLA Ops:
  0.6 0.8 copy.20
  1.4 0.8 reshape.34.parents_ref
  2.2 1.8 %copy.19.wg_ref = bf16[2048,16]{1,0:T(8,128)(2,1)} copy(bf16[2048,16]{0,1:T(8,128)(2,1)} %param.19) | data formatting | bytes 131072 | tf_op args[5]
  4.1 37.2 %project.1 = bf16[8,48,896]{2,1,0:T(8,128)(2,1)} custom-call(bf16[8,48,256]{2,1,0:T(8,128)(2,1)} %bitcast.9, f32[1,256]{1,0:T(1,128)} %bitcast.10, bf16[256,256]{1,0:T(8,128)(2,1)} %wq_ref.1, bf16[256,256]{1,0:T(8,128)(2,1)} %wk_ref.1, bf16[256,256]{1,0:T(8,128)(2,1)} %wv_ref.1, bf16[2048,16]{1,0:T(8,128)(2,1)} %copy.19.wg_ref, f32[1,16]{1,0:T(1,128)} %bitcast.11), custom_call_target="tpu_custom_call" | custom-call | tf_op jit(solution)/shard_map/project/pallas_call | solution.py:396
  41.3 20.1 %attend.1 = (bf16[24,512,256]{2,1,0:T(8,128)(2,1)}, bf16[24,512,256]{2,1,0:T(8,128)(2,1)}, bf16[384,384]{1,0:T(8,128)(2,1)}) custom-call(s32[24]{0:T(128)} %prior_s.1, s32[24]{0:T(128)} %accepted_s.1, bf16[384,896]{1,0:T(8,128)(2,1)} %bitcast.6, s32[384,1]{1,0:T(8,128)} %reshape.34.parents_ref, bf16[24,512,256]{2,1,0:T(8,128)(2,1)} %k_ref.1, ...), custom_call_target="tpu_custom_call" | custom-call | tf_op jit(solution)/shard_map/attend/pallas_call | solution.py:424
  61.4 26.5 %combine.1 = bf16[2,48,256]{2,1,0:T(8,128)(2,1)} custom-call(bf16[8,48,384]{2,1,0:T(8,128)(2,1)} %bitcast.7, bf16[256,256]{1,0:T(8,128)(2,1)} %w_ref.1), custom_call_target="tpu_custom_call" | custom-call | tf_op jit(solution)/shard_map/combine/pallas_call | solution.py:458
  87.9 1.4 %copy.23 = bf16[96,256]{1,0:T(8,128)(2,1)} copy(bf16[96,256]{1,0:T(8,128)(2,1)} %bitcast.8) | data formatting | bytes 98304

commit v2 on v1

--- a/solution.py
+++ b/solution.py
@@ -46,14 +46,14 @@
     bias_ref,
     out_ref,
     part,
+    swapped,
+    middle,
     arrived,
     gathered,
     mine,
-    send_a,
-    recv_a,
-    send_b,
-    recv_b,
+    *sems,
 ):
+    swap_sems, sum_sems, back_sems, last_sems = sems[0:2], sems[2:4], sems[4:6], sems[6:8]
     me = lax.axis_index("kv")
     tp = lax.axis_index("tp")
     chunk_rows, depth = tokens_ref.shape[1:]
@@ -64,17 +64,26 @@
             barrier, inc=1, device_id={"kv": lax.rem(me + d, n_kv)}, device_id_type=MESH
         )
 
-    total_heads = wg_ref.shape[1]
+    total_heads = bias_ref.shape[1]
     lane = iota((total_heads, LANES), 1)
     pick = (iota((total_heads, LANES), 0) == tp * heads + lane % 32) & (lane % 32 < heads) & (lane < 96)
     pick = jnp.where(pick, 1.0, 0.0)
-    gate_w = wg_ref[pl.ds(pl.multiple_of(me * depth, depth), depth), :]
-    gate_w = jnp.dot(gate_w, pick.astype(bf16), preferred_element_type=f32).astype(bf16)
+    if depth % LANES == 0:
+        slot = iota((LANES, total_heads), 0)
+        pick_rows = iota((LANES, total_heads), 1) == tp * heads + slot % 32
+        pick_rows = jnp.where(pick_rows & (slot % 32 < heads) & (slot < 96), 1.0, 0.0)
+        gate_w = wg_ref[:, pl.ds(pl.multiple_of(me * depth, depth), depth)]
+        gate_w = jnp.dot(pick_rows.astype(bf16), gate_w, preferred_element_type=f32).astype(bf16)
+        gate_product = functools.partial(contract_last, b=gate_w)
+    else:
+        gate_w = wg_ref[pl.ds(pl.multiple_of(me * depth, depth), depth), :]
+        gate_w = jnp.dot(gate_w, pick.astype(bf16), preferred_element_type=f32).astype(bf16)
+        gate_product = functools.partial(jnp.dot, b=gate_w, preferred_element_type=f32)
 
     def partial_sums(floats):
         scaled = (floats * gain_ref[...]).astype(bf16)
         square = jnp.sum(floats * floats, axis=1, keepdims=True)
-        gates = jnp.dot(scaled, gate_w, preferred_element_type=f32)
+        gates = gate_product(scaled)
         gates = jnp.where(iota(gates.shape, 1) == SQUARE_LANE, square, gates)
         products = [
             jnp.dot(scaled, w[...], preferred_element_type=f32).astype(bf16)
@@ -86,71 +95,111 @@
     if chunk_rows % 16 == 0:
         floats = tokens_ref[...].reshape(n_kv * chunk_rows, depth).astype(f32)
         for piece, low, high in zip(partial_sums(floats), edges[:-1], edges[1:]):
-            part[:, :, low:high] = piece.reshape(n_kv, chunk_rows, high - low)
+            blocks = piece.reshape(n_kv, chunk_rows, high - low)
+            for c in range(n_kv):
+                part[c % 2, c // 2, :, low:high] = blocks[c]
     else:
 
         def one(c, carry):
             for piece, low, high in zip(
                 partial_sums(tokens_ref[c].astype(f32)), edges[:-1], edges[1:]
             ):
-                part[c, :, low:high] = piece
+                part[lax.rem(c, 2), c // 2, :, low:high] = piece
             return carry
 
         lax.fori_loop(0, n_kv, one, 0)
 
+    outer = n_kv // 2
+    x, z = lax.rem(me, 2), me // 2
+    partner = me + 1 - 2 * x
+    pieces = [pl.ds(2 * width, width + LANES), pl.ds(0, width), pl.ds(width, width)]
+
+    def send(source, target, sems, at, device):
+        copy = pltpu.make_async_remote_copy(
+            src_ref=source,
+            dst_ref=target,
+            send_sem=sems[0].at[at],
+            recv_sem=sems[1].at[at],
+            device_id={"kv": device},
+            device_id_type=MESH,
+        )
+        copy.start()
+        return copy
+
     pl.semaphore_wait(barrier, n_kv - 1)
-    copies = []
-    for d in range(1, n_kv):
-        peer = lax.rem(me + d, n_kv)
-        copy = pltpu.make_async_remote_copy(
-            src_ref=part.at[peer],
-            dst_ref=arrived.at[d - 1],
-            send_sem=send_a.at[d - 1],
-            recv_sem=recv_a.at[d - 1],
-            device_id={"kv": peer},
-            device_id_type=MESH,
-        )
-        copy.start()
-        copies.append(copy)
-    total = part[me].astype(f32)
-    for d in range(1, n_kv):
-        copies[d - 1].wait_recv()
-        total = total + arrived[d - 1].astype(f32)
-    tail = total[:, 3 * width :]
-    tail_lane = iota(tail.shape, 1)
-    square = jnp.sum(jnp.where(tail_lane == SQUARE_LANE, tail, 0.0), axis=1, keepdims=True)
-    inv_rms = lax.rsqrt(square / (n_kv * depth) + norm_eps)
+    swaps = [
+        send(part.at[1 - x, :, :, at], swapped.at[:, :, at], swap_sems, p, partner)
+        for p, at in enumerate(pieces)
+    ]
+    sums = []
+    for p, at in enumerate(pieces):
+        swaps[p].wait_recv()
+        half = part[x, :, :, at].astype(f32) + swapped[:, :, at].astype(f32)
+        middle[:, :, at] = half.astype(bf16)
+        row = []
+        for d in range(1, outer):
+            other = lax.rem(z + d, outer)
+            row.append(
+                send(
+                    middle.at[other, :, at],
+                    arrived.at[d - 1, :, at],
+                    sum_sems,
+                    p * (outer - 1) + d - 1,
+                    other * 2 + x,
+                )
+            )
+        sums.append(row)
     bias = jnp.dot(
         jnp.broadcast_to(bias_ref[...], (8, total_heads)),
         pick,
         preferred_element_type=f32,
         precision=HIGHEST,
     )[0:1]
-    pre = inv_rms * tail + bias
-    log_gates = jnp.minimum(pre, 0.0) - jnp.log1p(jnp.exp(-jnp.abs(pre)))
-    hi, mid, low = split3(log_gates)
-    packed = jnp.where(tail_lane < 32, hi, jnp.where(tail_lane < 64, mid, low))
-    packed = jnp.where((tail_lane % 32 < heads) & (tail_lane < 96), packed, 0.0)
-    mine[:, : 3 * width] = (inv_rms * total[:, : 3 * width]).astype(bf16)
-    mine[:, 3 * width :] = packed.astype(bf16)
-    back = []
-    for d in range(1, n_kv):
-        copy = pltpu.make_async_remote_copy(
-            src_ref=mine,
-            dst_ref=gathered.at[me],
-            send_sem=send_b.at[d - 1],
-            recv_sem=recv_b.at[d - 1],
-            device_id={"kv": lax.rem(me + d, n_kv)},
-            device_id_type=MESH,
-        )
-        copy.start()
-        back.append(copy)
-    out_ref[me] = mine[...]
-    for d in range(1, n_kv):
-        source = lax.rem(me + n_kv - d, n_kv)
-        back[d - 1].wait_recv()
-        out_ref[source] = gathered[source]
-    for copy in copies + back:
+    inv_rms = None
+    backs = []
+    for p, at in enumerate(pieces):
+        total = middle[z, :, at].astype(f32)
+        for d in range(1, outer):
+            sums[p][d - 1].wait_recv()
+            total = total + arrived[d - 1, :, at].astype(f32)
+        if p == 0:
+            tail = total[:, width:]
+            tail_lane = iota(tail.shape, 1)
+            square = jnp.sum(jnp.where(tail_lane == SQUARE_LANE, tail, 0.0), axis=1, keepdims=True)
+            inv_rms = lax.rsqrt(square / (n_kv * depth) + norm_eps)
+            pre = inv_rms * tail + bias
+            log_gates = jnp.minimum(pre, 0.0) - jnp.log1p(jnp.exp(-jnp.abs(pre)))
+            hi, mid, low = split3(log_gates)
+            packed = jnp.where(tail_lane < 32, hi, jnp.where(tail_lane < 64, mid, low))
+            packed = jnp.where((tail_lane % 32 < heads) & (tail_lane < 96), packed, 0.0)
+            mine[:, 3 * width :] = packed.astype(bf16)
+            total = total[:, :width]
+        mine[:, pl.ds(at.start, width)] = (inv_rms * total).astype(bf16)
+        backs.append(
+            [
+                send(
+                    mine.at[:, at],
+                    gathered.at[x, z, :, at],
+                    back_sems,
+                    p * (outer - 1) + d - 1,
+                    lax.rem(z + d, outer) * 2 + x,
+                )
+                for d in range(1, outer)
+            ]
+        )
+        gathered[x, z, :, at] = mine[:, at]
+    lasts = []
+    for p, at in enumerate(pieces):
+        for copy in backs[p]:
+            copy.wait_recv()
+        lasts.append(
+            send(gathered.at[x, :, :, at], gathered.at[x, :, :, at], last_sems, p, partner)
+        )
+    for copy in lasts:
+        copy.wait_recv()
+    for c in range(n_kv):
+        out_ref[c] = gathered[c % 2, c // 2]
+    for copy in swaps + sum(sums, []) + sum(backs, []) + lasts:
         copy.wait_send()
 
 
@@ -167,7 +216,18 @@
 
     row = iota((rows, rows), 0)
     column = iota((rows, rows), 1)
-    parent = parents_ref[...]
+    every = parents_ref[...]
+    parent = jnp.concatenate(
+        [
+            jnp.sum(
+                jnp.where(iota(every.shape, 1) == step * group + b, every, 0).astype(f32),
+                axis=1,
+                keepdims=True,
+            ).astype(i32)
+            for b in range(group)
+        ],
+        axis=0,
+    )
     link = (parent + (row // PROPS) * PROPS == column) & (parent >= 0)
     reached = jnp.where(link | (row == column), 1.0, 0.0)
     for squaring in range((PROPS - 1).bit_length()):
@@ -399,12 +459,16 @@
         in_specs=[vmem] * 7,
         out_specs=vmem,
         scratch_shapes=[
-            pltpu.VMEM((n_kv, chunk_rows, proj_width), bf16),
-            pltpu.VMEM((n_kv - 1, chunk_rows, proj_width), bf16),
-            pltpu.VMEM((n_kv, chunk_rows, proj_width), bf16),
+            pltpu.VMEM((2, n_kv // 2, chunk_rows, proj_width), bf16),
+            pltpu.VMEM((n_kv // 2, chunk_rows, proj_width), bf16),
+            pltpu.VMEM((n_kv // 2, chunk_rows, proj_width), bf16),
+            pltpu.VMEM((n_kv // 2 - 1, chunk_rows, proj_width), bf16),
+            pltpu.VMEM((2, n_kv // 2, chunk_rows, proj_width), bf16),
             pltpu.VMEM((chunk_rows, proj_width), bf16),
         ]
-        + [dma((n_kv - 1,))] * 4,
+        + [dma((3,))] * 2
+        + [dma((3 * (n_kv // 2 - 1),))] * 4
+        + [dma((3,))] * 2,
         compiler_params=pltpu.CompilerParams(collective_id=0, has_side_effects=True),
         name="project",
     )(
@@ -413,7 +477,7 @@
         w_query,
         w_key,
         w_value,
-        w_gate,
+        w_gate.T if depth % LANES == 0 else w_gate,
         gate_bias.reshape(1, -1),
     )
     projected = projected.reshape(row_count, proj_width)
@@ -433,7 +497,7 @@
             grid=(seq_count // group,),
             in_specs=[
                 pl.BlockSpec((rows, proj_width), lambda s, *_: (s, 0)),
-                pl.BlockSpec((rows, 1), lambda s, *_: (s, 0)),
+                pl.BlockSpec((PROPS, seq_count), lambda s, *_: (0, 0)),
                 cache_spec,
                 cache_spec,
                 pl.BlockSpec((group, heads, length), lambda s, *_: (s, 0, 0)),
@@ -449,7 +513,7 @@
         prior_len,
         accepted,
         projected,
-        parents.reshape(row_count, 1),
+        parents.T,
         keys_cache,
         values_cache,
         cum_gates,

time: 89.6 us -> 79.4 us (0.89)
  Pallas kernels: 83.8 us -> 77.1 us
  local copies, waits for them, and re-layouts: 4.85 us -> 1.42 us
    pallas_call x1, Pallas kernels: 37.2 us -> 33.5 us  [shards(): pl.pallas_call(functools.partial(project_kernel, n_kv, heads), out_shape=...]
    pallas_call x1, Pallas kernels: 26.5 us -> 22.7 us  [shards(): pl.pallas_call(functools.partial(combine_kernel, n_kv, n_tp, heads), out_...]
    unnamed x3 -> x1, local copies, waits for them, and re-layouts: 4.03 us -> 1.42 us
where the time goes in v2:
time: 79.4 us; the launch traced here: 79.2 us
  Pallas kernels  77.1 us (97%)
  local copies, waits for them, and re-layouts  1.42 us (2%)
    pallas_call x1, Pallas kernels, shards(): pl.pallas_call(functools.partial(project_kernel, n_kv, heads), out_shape=...  33.5 us
    pallas_call x1, Pallas kernels, shards(): pl.pallas_call(functools.partial(combine_kernel, n_kv, n_tp, heads), out_...  22.7 us
    pallas_call x1, Pallas kernels, shards(): pl.pallas_call(functools.partial(attend_kernel, heads), out_shape=(jax.Sh...  20.9 us

profile of v2, /device:TPU:0, one launch (start us, length us, event | category | flops | bytes accessed | tf_op | source)
XLA Modules:
  0.0 79.2 jit_solution(13368057750281725534)
XLA Ops:
  0.6 33.5 %project.1 = bf16[8,48,896]{2,1,0:T(8,128)(2,1)} custom-call(bf16[8,48,256]{2,1,0:T(8,128)(2,1)} %bitcast.11, f32[1,256]{1,0:T(1,128)} %bitcast.14, bf16[256,256]{1,0:T(8,128)(2,1)} %wq_ref.1, bf16[256,256]{1,0:T(8,128)(2,1)} %wk_ref.1, bf16[256,256]{1,0:T(8,128)(2,1)} %wv_ref.1, bf16[16,2048]{1,0:T(8,128)(2,1)} %bitcast.12, f32[1,16]{1,0:T(1,128)} %bitcast.15), custom_call_target="tpu_custom_call" | custom-call | tf_op jit(solution)/shard_map/project/pallas_call | solution.py:456
  34.1 20.9 %attend.1 = (bf16[24,512,256]{2,1,0:T(8,128)(2,1)}, bf16[24,512,256]{2,1,0:T(8,128)(2,1)}, bf16[384,384]{1,0:T(8,128)(2,1)}) custom-call(s32[24]{0:T(128)} %prior_s.1, s32[24]{0:T(128)} %accepted_s.1, bf16[384,896]{1,0:T(8,128)(2,1)} %bitcast.8, s32[16,24]{1,0:T(8,128)} %bitcast.13, bf16[24,512,256]{2,1,0:T(8,128)(2,1)} %k_ref.1, ...), custom_call_target="tpu_custom_call" | custom-call | tf_op jit(solution)/shard_map/attend/pallas_call | solution.py:488
  55.0 22.7 %combine.1 = bf16[2,48,256]{2,1,0:T(8,128)(2,1)} custom-call(bf16[8,48,384]{2,1,0:T(8,128)(2,1)} %bitcast.9, bf16[256,256]{1,0:T(8,128)(2,1)} %w_ref.1), custom_call_target="tpu_custom_call" | custom-call | tf_op jit(solution)/shard_map/combine/pallas_call | solution.py:522
  77.8 1.4 %copy.18 = bf16[96,256]{1,0:T(8,128)(2,1)} copy(bf16[96,256]{1,0:T(8,128)(2,1)} %bitcast.10) | data formatting | bytes 98304
